TPU v7x, 256 devices: a whole 4x4x8 slice. The times are simulated.
256 devices in a mesh: ep: 16 (over y, x), tp: 16 (over z, core).
Axes of the slice: x: 4, y: 4, z: 8, core: 2. Of those that a mesh axis runs over, the one named last changes fastest.
Arguments:
- pool_in: bfloat16 [131072, 1024], P(('ep', 'tp')), may hold values from -6 to 6
- pool_weight: bfloat16 [4, 256, 256], replicated, may hold values from -0.375 to 0.375
- pool_gain: float32 [1024], replicated, may hold values from 0.1 to 1.9
- out_weight: bfloat16 [1024, 2048], P('tp'), may hold values from -0.1875 to 0.1875
- mix_gain: float32 [2048], replicated, may hold values from 0.1 to 1.9
- expert_in: bfloat16 [4096, 2048], P('ep'), may hold values from -6 to 6
- routes: int32 [4096, 4], P('ep'), may hold values from 0 to 31, all different within a row; in each aligned block of 16 rows (0 to 15, 16 to 31, ...) at most 4 rows name the same one
- route_weight: float32 [4096, 4], P('ep'), may hold values from 0.1 to 1
- pre_gain: float32 [2048], replicated, may hold values from 0.1 to 1.9
- gate_weight: bfloat16 [32, 2048, 4096], P('ep', None, 'tp'), may hold values from -0.39648438 to 0.39648438
- up_weight: bfloat16 [32, 2048, 4096], P('ep', None, 'tp'), may hold values from -0.39648438 to 0.39648438
- down_weight: bfloat16 [32, 4096, 2048], P('ep', 'tp'), may hold values from -0.09375 to 0.09375
- post_gain: float32 [2048], replicated, may hold values from 0.1 to 1.9
Outputs:
- mix_out: bfloat16 [131072, 2048], P(('ep', 'tp'))
- expert_out: bfloat16 [4096, 2048], P(('ep', 'tp'))
Inputs may be any that keep to these rules, and one draw needn't show every extreme that they name: `routes`: each row names 4 different experts. In each aligned block of 16 rows no expert is named by more than 4 rows, a bound that some block reaches.
All inputs are finite; a program needn't handle non-finite values.
Results may differ from a plain program's by a relative error of at most 0.019.
Values may be sent and summed in bfloat16 or wider, within the bound.
A program may use at most 128 MiB of HBM per device.

v0:
```python
import jax
import jax.numpy as jnp
from jax import lax
from jax.sharding import PartitionSpec as P

WINDOWS = (2, 4, 8, 16)
EPS = 1e-06
LIMIT = 7.0
ALPHA = 1.702


def shifted(block, axis, distance):
    devices = range(lax.axis_size(axis))
    route = [(i - distance, i) for i in devices if i - distance in devices]
    return lax.ppermute(block, axis, route)


def rms_scale(values, gain):
    mean_square = jnp.mean(values * values, axis=-1, keepdims=True)
    return values * lax.rsqrt(mean_square + EPS) * gain


def trailing_pool(padded, first_pos, rows):
    group = padded.shape[1] // 4
    position = first_pos + jnp.arange(rows, dtype=jnp.int32)
    pieces = []
    for which, window in enumerate(WINDOWS):
        channels = padded[:, which * group : (which + 1) * group]
        running = channels[16 : 16 + rows]
        for reach in range(2, window + 1):
            running = running + channels[17 - reach : 17 - reach + rows]
        count = jnp.minimum(position + 1, window).astype(jnp.float32)[:, None]
        pieces.append(running / count)
    pooled = jnp.concatenate(pieces, axis=1)
    return (pooled - padded[16:]).astype(jnp.bfloat16)


def selection(block_routes, experts, capacity):
    flat = block_routes.reshape(-1)
    onehot = (flat[:, None] == jnp.arange(experts, dtype=jnp.int32)[None, :]).astype(jnp.int32)
    earlier = jnp.cumsum(onehot, axis=0) - onehot
    rank = jnp.sum(earlier * onehot, axis=1)
    slots = (flat * capacity + rank).reshape(block_routes.shape)
    return (
        slots[:, :, None] == jnp.arange(experts * capacity, dtype=jnp.int32)[None, None, :]
    ).astype(jnp.bfloat16)


def clamped_unit(gate, up):
    gate = jnp.minimum(gate, LIMIT)
    up = jnp.clip(up, -LIMIT, LIMIT)
    return (up + 1.0) * gate * jax.nn.sigmoid(ALPHA * gate)


def hidden_rows(arrived, gate_weight, up_weight):
    gate = jnp.einsum("necd,edf->necf", arrived, gate_weight, preferred_element_type=jnp.float32)
    up = jnp.einsum("necd,edf->necf", arrived, up_weight, preferred_element_type=jnp.float32)
    return clamped_unit(gate, up).astype(jnp.bfloat16)


def body(
    pool_in,
    pool_weight,
    pool_gain,
    out_weight,
    mix_gain,
    expert_in,
    routes,
    route_weight,
    pre_gain,
    gate_weight,
    up_weight,
    down_weight,
    post_gain,
):
    rows, channels = pool_in.shape
    width = out_weight.shape[1]
    rim = shifted(pool_in[rows - 16 :], ("ep", "tp"), 1)
    padded = jnp.concatenate([rim, pool_in], axis=0).astype(jnp.float32)
    first_pos = (lax.axis_index("ep") * lax.axis_size("tp") + lax.axis_index("tp")) * rows
    diff = trailing_pool(padded, first_pos, rows)
    mixed = jnp.einsum(
        "sgc,gcd->sgd",
        diff.reshape(rows, 4, channels // 4),
        pool_weight,
        preferred_element_type=jnp.float32,
    )
    mixed = (mixed.reshape(rows, channels) * pool_gain).astype(jnp.bfloat16)
    projected = jnp.dot(
        mixed,
        lax.all_gather(out_weight, "tp", axis=0, tiled=True),
        preferred_element_type=jnp.float32,
    )
    mix_out = rms_scale(projected, mix_gain).astype(jnp.bfloat16)
    ep_count = lax.axis_size("ep")
    tp_count = lax.axis_size("tp")
    tp_place = lax.axis_index("tp")
    local_experts = gate_weight.shape[0]
    experts = local_experts * ep_count
    tokens_here, choose = routes.shape
    block_tokens = tokens_here // tp_count
    capacity = 2 * block_tokens * choose // experts
    block_routes = lax.dynamic_slice_in_dim(routes, tp_place * block_tokens, block_tokens, 0)
    block_rows = lax.dynamic_slice_in_dim(expert_in, tp_place * block_tokens, block_tokens, 0)
    normed = rms_scale(block_rows.astype(jnp.float32), pre_gain).astype(jnp.bfloat16)
    own_picks = selection(block_routes, experts, capacity)
    buffer = jnp.einsum(
        "ts,td->sd", jnp.sum(own_picks, axis=1), normed, preferred_element_type=jnp.float32
    ).astype(jnp.bfloat16)
    buffer = buffer.reshape(ep_count, local_experts, capacity, width)
    arrived = lax.all_to_all(buffer, "ep", split_axis=0, concat_axis=0, tiled=True)
    hidden_all = hidden_rows(
        lax.all_gather(arrived, "tp", axis=0, tiled=True), gate_weight, up_weight
    )
    summed = lax.psum_scatter(
        jnp.einsum(
            "necf,efd->necd", hidden_all, down_weight, preferred_element_type=jnp.float32
        ).astype(jnp.bfloat16),
        "tp",
        scatter_dimension=0,
        tiled=True,
    )
    returned = lax.all_to_all(summed, "ep", split_axis=0, concat_axis=0, tiled=True)
    returned = returned.reshape(experts * capacity, width)
    per_route = jnp.einsum("tks,sd->tkd", own_picks, returned, preferred_element_type=jnp.float32)
    weights = lax.dynamic_slice_in_dim(route_weight, tp_place * block_tokens, block_tokens, 0)
    combined = jnp.sum(per_route * weights[:, :, None], axis=1)
    expert_out = rms_scale(combined, post_gain).astype(jnp.bfloat16)
    return (mix_out, expert_out)


def solution(mesh):
    return jax.shard_map(
        body,
        mesh=mesh,
        in_specs=(
            P(("ep", "tp"), None),
            P(),
            P(),
            P("tp", None),
            P(),
            P("ep", None),
            P("ep", None),
            P("ep", None),
            P(),
            P("ep", None, "tp"),
            P("ep", None, "tp"),
            P("ep", "tp", None),
            P(),
        ),
        out_specs=(P(("ep", "tp"), None), P(("ep", "tp"), None)),
        check_vma=False,
    )
```

profile of v0, /device:TPU:1, one launch (start us, length us, event | category | flops | bytes accessed | tf_op | source)
XLA Modules:
  0.0 223.9 jit_solution(3929934778981282505)
XLA Ops:
  7.2 0.0 copy-start
  7.2 0.0 all-gather.5.cloned.1.call-start
  7.2 0.9 constant_dynamic-slice_fusion.1
  8.1 0.1 copy.36
  8.2 0.1 eq.28
  8.3 0.1 fusion.34
  8.4 0.1 reduce_window_sum.11
  8.5 0.2 select_reduce_fusion
  8.7 0.1 reduce_sum.61
  8.8 0.1 copy.29
  8.8 0.1 fusion.35
  8.9 1.0 fusion.26
  9.9 1.2 convolution_convert_fusion
  11.1 0.2 reshape.74
  11.3 17.8 %all_to_all.10 = bf16[16,2,4,2048]{3,2,1,0:T(4,128)(2,1)S(1)} all-to-all(bf16[16,2,4,2048]{3,2,1,0:T(4,128)(2,1)S(1)} %reshape.74), channel_id=1, replica_groups=mesh['ep'=16,'tp'=16] {'ep'}, dimensions={0} | all-to-all | bytes 1048576 | tf_op jit(solution)/shard_map/all_to_all | solution.py:111
  29.1 1.1 copy.30
  30.2 0.0 all-gather.5.cloned.1.call-update
  30.2 0.0 all-gather.3.cloned.1.call-start
  30.3 0.7 all-gather.3.cloned.1.call-update
  31.0 0.0 reduce-scatter.2.cloned.1.call-start
  31.0 56.1 %all-gather.5.cloned.1.call-done = bf16[256,2,4,2048]{3,0,2,1:T(8,128)(2,1)} async-done(((bf16[16,2,4,2048]{3,0,2,1:T(8,128)(2,1)}), bf16[256,2,4,2048]{3,0,2,1:T(8,128)(2,1)}) %all-gather.5.cloned.1.call-update) | async-done | bytes 8388624 | tf_op jit(solution)/shard_map/all_gather | solution.py:113
  87.1 7.6 %fusion.4 = f32[2,256,4,256]{3,1,2,0:T(8,128)} fusion(bf16[256,2,4,2048]{3,0,2,1:T(8,128)(2,1)} %all-gather.5.cloned.1.call-done, bf16[2,2048,256]{2,1,0:T(8,128)(2,1)} %param.23), kind=kOutput, calls=%fused_computation.10 | convolution fusion | flops 2147483648 | bytes 12582912 | tf_op jit(solution)/shard_map/necd,edf->necf/dot_general | solution.py:57
  94.7 0.0 copy-done
  94.7 13.7 %convert_bitcast_fusion = bf16[256,2,4,2048]{3,0,2,1:T(8,128)(2,1)} fusion(bf16[2,256,2048]{2,1,0:T(8,128)(2,1)S(1)} %copy-done, bf16[256,2,4,2048]{3,0,2,1:T(8,128)(2,1)} %all-gather.5.cloned.1.call-done, bf16[2,2048,256]{2,1,0:T(8,128)(2,1)} %param.22, f32[2,256,4,256]{3,1,2,0:T(8,128)} %fusion.4), kind=kOutput, calls=%fused_computation | convolution fusion | flops 4304404480 | bytes 23068672 | tf_op jit(solution)/shard_map/necf,efd->necd/dot_general | solution.py:116
  108.5 0.0 copy-start.1
  108.5 0.0 copy-start.6
  108.5 0.0 reduce-scatter.2.cloned.1.call-update
  108.5 1.2 copy-done.1
  109.7 2.1 collective-permute-start
  111.8 0.0 copy-done.6
  111.9 0.1 constant_dynamic-slice_fusion
  111.9 1.0 collective-permute-done
  112.9 0.2 maximum_convert_fusion
  113.1 0.6 fusion.22
  113.8 0.6 fusion.25
  114.4 0.0 copy-start.2
  114.4 0.4 fusion
  114.9 0.0 copy-start.5
  114.9 0.6 copy-done.2
  115.5 0.5 fusion.15
  116.0 0.0 copy-done.5
  116.0 0.2 fusion.6
  116.2 13.3 %all-gather.3.cloned.1.call-done = bf16[1024,2048]{1,0:T(8,128)(2,1)} async-done(((bf16[64,2048]{1,0:T(8,128)(2,1)}), bf16[1024,2048]{1,0:T(8,128)(2,1)}) %all-gather.3.cloned.1.call-update) | async-done | bytes 4194320 | tf_op jit(solution)/shard_map/all_gather | solution.py:91
  129.5 6.6 %multiply_reduce_fusion = (f32[512]{0:T(512)S(1)}, f32[512,2048]{1,0:T(8,128)}) fusion(bf16[512,1024]{0,1:T(8,128)(2,1)S(1)} %fusion.6, bf16[1024,2048]{1,0:T(8,128)(2,1)} %all-gather.3.cloned.1.call-done), kind=kOutput, calls=%fused_computation.2 | convolution fusion | flops 2149580288 | bytes 9439232 | tf_op jit(solution)/shard_map/dot_general | solution.py:89
  136.1 0.0 copy-start.3
  136.1 62.0 %reduce-scatter.2.cloned.1.call-done = bf16[16,2,4,2048]{3,0,2,1:T(8,128)(2,1)} async-done(((bf16[256,2,4,2048]{3,0,2,1:T(8,128)(2,1)}), bf16[16,2,4,2048]{3,0,2,1:T(8,128)(2,1)}) %reduce-scatter.2.cloned.1.call-update) | async-done | bytes 524304 | tf_op jit(solution)/shard_map/reduce_scatter | solution.py:115
  198.1 2.2 copy.31
  200.4 6.5 %all-to-all-start.1 = ((bf16[16,2,4,2048]{3,2,1,0:T(4,128)(2,1)}), bf16[16,2,4,2048]{3,2,1,0:T(4,128)(2,1)S(1)}, u32[]{:S(2)}, u32[]{:S(2)}) async-start(bf16[16,2,4,2048]{3,2,1,0:T(4,128)(2,1)} %copy.31), calls=%async_computation.2 | async-start | bytes 1048576 | tf_op jit(solution)/shard_map/all_to_all | solution.py:123
  206.9 0.0 copy-done.3
  206.9 0.0 copy-start.4
  206.9 3.9 %multiply_convert_fusion = bf16[512,2048]{1,0:T(8,128)(2,1)} fusion(f32[512,2048]{1,0:T(8,128)} %get-tuple-element.6, f32[2048]{0:T(1024)S(1)} %copy-done.3, f32[512]{0:T(512)S(1)} %add_rsqrt_fusion), kind=kLoop, calls=%fused_computation.1 | loop fusion | flops 3145728 | bytes 6301696 | tf_op jit(solution)/shard_map/convert_element_type | solution.py:94
  210.8 5.3 %all-to-all-done.1 = bf16[16,2,4,2048]{3,2,1,0:T(4,128)(2,1)S(1)} async-done(((bf16[16,2,4,2048]{3,2,1,0:T(4,128)(2,1)}), bf16[16,2,4,2048]{3,2,1,0:T(4,128)(2,1)S(1)}, u32[]{:S(2)}, u32[]{:S(2)}) %all-to-all-start.1) | async-done | bytes 524320 | tf_op jit(solution)/shard_map/all_to_all | solution.py:123
  216.1 0.1 reshape.79
  216.3 0.3 fusion.14
  216.6 0.1 multiply_reduce_fusion.1
  216.7 0.0 copy-done.4
  216.7 0.7 multiply_convert_fusion.2
  (7 shorter events, 0.1 us)
Async XLA Ops:
  7.2 87.6 %copy-start = (bf16[2,256,2048]{2,1,0:T(8,128)(2,1)S(1)}, bf16[2,256,2048]{2,1,0:T(8,128)(2,1)}, u32[]{:S(2)}) copy-start(bf16[2,256,2048]{2,1,0:T(8,128)(2,1)} %param.24) | copy-start | bytes 6291460
  7.2 79.9 %all-gather.5.cloned.1.call-start = ((), (), s32[]{:S(2)}) async-start(), calls=%async_computation.4 | async-start | bytes 8912896 | tf_op jit(solution)/shard_map/all_gather | solution.py:113
  30.2 99.3 %all-gather.3.cloned.1.call-start = ((), (), s32[]{:S(2)}) async-start(), calls=%async_computation.3 | async-start | bytes 4456448 | tf_op jit(solution)/shard_map/all_gather | solution.py:91
  31.0 167.1 %reduce-scatter.2.cloned.1.call-start = ((), (), s32[]{:S(2)}) async-start(), calls=%async_computation.5 | async-start | bytes 8912896 | tf_op jit(solution)/shard_map/reduce_scatter | solution.py:115
  108.5 1.2 copy-start.1
  108.5 3.4 %copy-start.6 = (f32[256,4]{0,1:T(4,128)S(1)}, f32[256,4]{0,1:T(4,128)}, u32[]{:S(2)}) copy-start(f32[256,4]{0,1:T(4,128)} %param.20) | copy-start | bytes 12292
  109.7 3.2 %collective-permute-start = (bf16[16,1024]{1,0:T(8,128)(2,1)S(1)}, bf16[16,1024]{1,0:T(8,128)(2,1)S(1)}, u32[]{:S(2)}, u32[]{:S(2)}) collective-permute-start(bf16[16,1024]{1,0:T(8,128)(2,1)S(1)} %slice.130), channel_id=1, source_target_pairs={{0,1},{1,2},{2,3},{3,4},{4,5},{5,6},{6,7},{7,8},{8,9},{9,10},{10,1... | collective-permute-start | bytes 98312 | tf_op jit(solution)/shard_map/ppermute | solution.py:15
  114.4 1.0 copy-start.2
  114.9 1.1 copy-start.5
  136.1 70.8 %copy-start.3 = (f32[2048]{0:T(1024)S(1)}, f32[2048]{0:T(1024)}, u32[]{:S(2)}) copy-start(f32[2048]{0:T(1024)} %param.17) | copy-start | bytes 24580
  200.4 15.8 %all-to-all-start.1 = ((bf16[16,2,4,2048]{3,2,1,0:T(4,128)(2,1)}), bf16[16,2,4,2048]{3,2,1,0:T(4,128)(2,1)S(1)}, u32[]{:S(2)}, u32[]{:S(2)}) async-start(bf16[16,2,4,2048]{3,2,1,0:T(4,128)(2,1)} %copy.31), calls=%async_computation.2 | async-start | bytes 1048576 | tf_op jit(solution)/shard_map/all_to_all | solution.py:123
  206.9 9.8 %copy-start.4 = (f32[2048]{0:T(1024)S(1)}, f32[2048]{0:T(1024)}, u32[]{:S(2)}) copy-start(f32[2048]{0:T(1024)} %param.25) | copy-start | bytes 24580
Sparse Core Ops, SparseCore 0:
  30.3 56.7 all-gather.4
  88.9 40.4 all-gather.2
  132.0 66.0 reduce-scatter.1
where the time goes:
time: 227 us; the launch traced here: 224 us
  waiting for transfers between devices  138 us (61%)
  matrix products  29.9 us (13%)
  blocking collectives  17.8 us (8%)
  between operations  13.9 us (6%)
  starting transfers between devices  8.73 us (4%)
  other arithmetic  8.4 us (4%)
  local copies, waits for them, and re-layouts  6.76 us (3%)
    reduce_scatter x1, waiting for transfers between devices, body(): lax.psum_scatter(jnp.einsum('necf,efd->necd', hidden_all, down_weight, pr...  62 us
    all_gather x1, waiting for transfers between devices, body(): lax.all_gather(arrived, 'tp', axis=0, tiled=True)  56.1 us
    all_to_all x1, blocking collectives, body(): lax.all_to_all(buffer, 'ep', split_axis=0, concat_axis=0, tiled=True)  17.8 us
    dot_general x1, matrix products, body(): jnp.einsum('necf,efd->necd', hidden_all, down_weight, preferred_element_t...  13.7 us
    all_gather x1, waiting for transfers between devices, body(): lax.all_gather(out_weight, 'tp', axis=0, tiled=True)  13.3 us
    dot_general x1, matrix products, hidden_rows(): jnp.einsum('necd,edf->necf', arrived, up_weight, preferred_element_type=j...  7.62 us
    dot_general x1, matrix products, body(): jnp.dot(mixed, lax.all_gather(out_weight, 'tp', axis=0, tiled=True), pref...  6.59 us
    all_to_all x1, starting transfers between devices, body(): lax.all_to_all(summed, 'ep', split_axis=0, concat_axis=0, tiled=True)  6.52 us
  transfers between devices with their start and end apart: 5, of which 5 were waited for; matrix products, arithmetic and copies ran while one was open for 15% of the time, Pallas kernels for 0%

commit v1 on v0

v1 whole, which is shorter than its diff:
```python
import functools

import jax
import jax.numpy as jnp
from jax import lax
from jax.experimental import pallas as pl
from jax.experimental.pallas import tpu as pltpu
from jax.sharding import PartitionSpec as P

MESH = pl.DeviceIdType.MESH
WINDOWS = (2, 4, 8, 16)
EPS = 1e-06
LIMIT = 7.0
ALPHA = 1.702
F32 = jnp.float32
BF16 = jnp.bfloat16


def ring(a):
    return min(a, 4 - a)


ORDER = sorted(((a, b) for a in range(4) for b in range(4)), key=lambda t: ring(t[0]) + ring(t[1]))


def clamped_unit(gate, up):
    gate = jnp.minimum(gate, LIMIT)
    up = jnp.clip(up, -LIMIT, LIMIT)
    return (up + 1.0) * gate * jax.nn.sigmoid(ALPHA * gate)


def remote(src, dst, send, recv, device):
    return pltpu.make_async_remote_copy(
        src_ref=src, dst_ref=dst, send_sem=send, recv_sem=recv, device_id=device, device_id_type=MESH
    )


def kernel(
    pool_in, pool_weight, pool_gain, out_weight, mix_gain, expert_in, routes, route_weight, pre_gain,
    gate_weight, up_weight, down_weight, post_gain,
    mix_out, expert_out,
    xin, sendbuf, rows_in, rows_z, part_in, part_z, sums, neigh, back, mine, theirs,
    gate_w, up_w, down_w, padded, mixed, w_all, acc, staged,
    local_sem, send_a, recv_a, send_z, recv_z, send_p, recv_p, send_r, recv_r, send_t, recv_t,
    send_w, recv_w, send_o, recv_o, send_h, recv_h, out_sem,
):
    i = lax.axis_index("ep")
    j = lax.axis_index("tp")
    z, c = j // 2, j % 2
    y, x = i // 4, i % 4
    p = z % 2
    here = (i, j)
    mate = (i, 2 * z + 1 - c)

    def plane(dy, dx):
        return ((y + dy) % 4) * 4 + (x + dx) % 4

    def along(dz):
        return (i, 2 * ((z + dz) % 8) + c)

    after = (jnp.where(j == 15, (i + 1) % 16, i), (j + 1) % 16)
    before = (jnp.where(j == 0, (i + 15) % 16, i), (j + 15) % 16)

    def block_row(parity, b):
        return pl.multiple_of((2 * (parity + 2 * b) + c) * 16, 16)

    loads = []

    def load(src, dst):
        copy = pltpu.make_async_copy(src, dst, local_sem.at[len(loads)])
        copy.start()
        loads.append(copy)
        return copy

    token_loads = [
        load(expert_in.at[pl.ds(block_row(1 - p, b), 16)], xin.at[pl.ds(16 * b, 16)]) for b in range(4)
    ]
    weight_loads = [
        load(gate_weight.at[c], gate_w.at[0]),
        load(up_weight.at[c], up_w.at[0]),
        load(down_weight.at[c], down_w.at[0]),
    ]
    pool_load = load(pool_in, padded.at[pl.ds(16, 512)])
    slow, fast = jnp.where(c == 0, y, x), jnp.where(c == 0, x, y)
    w_mine = slow * 4 + fast
    w_src = out_weight.at[:, pl.ds(pl.multiple_of(i * 128, 128), 128)]
    w_load = load(w_src, w_all.at[c, w_mine, z])

    bar = pltpu.get_barrier_semaphore()

    def greet(device):
        pl.semaphore_signal(bar, inc=1, device_id=device, device_id_type=MESH)

    for dy, dx in ORDER[1:]:
        for core in range(2):
            greet((plane(dy, dx), 2 * z + core))
    for dz in range(1, 8):
        greet(along(dz))
    greet(mate)
    greet((jnp.where(c == 1, after[0], before[0]), jnp.where(c == 1, after[1], before[1])))

    lane = lax.broadcasted_iota(jnp.int32, (1, 512), 1)
    expert = jnp.zeros((1, 512), jnp.int32)
    for k, (dy, dx) in enumerate(ORDER):
        expert = jnp.where(lane // 32 == k, 2 * plane(dy, dx), expert)
    expert = expert + (lane // 16) % 2
    slot_lane = lane % 16
    token = lax.broadcasted_iota(jnp.int32, (64, 64), 0)
    other = lax.broadcasted_iota(jnp.int32, (64, 64), 1)
    earlier = jnp.where((other < token) & (other // 16 == token // 16), 1.0, 0.0).astype(BF16)
    base = (lax.broadcasted_iota(jnp.int32, (64, 1), 0) // 16) * 4

    def selection(parity, weighted):
        chosen = jnp.concatenate([routes[pl.ds(block_row(parity, b), 16), :] for b in range(4)], axis=0)
        weights = jnp.concatenate([route_weight[pl.ds(block_row(parity, b), 16), :] for b in range(4)], axis=0)
        hot = jnp.zeros((64, 512), F32)
        value = jnp.zeros((64, 512), F32)
        for k in range(4):
            match = chosen[:, k : k + 1] == expert
            hot = jnp.where(match, 1.0, hot)
            value = jnp.where(match, weights[:, k : k + 1], value)
        rank = jnp.dot(earlier, hot.astype(BF16), preferred_element_type=F32).astype(jnp.int32)
        taken = (rank + base) == slot_lane
        return jnp.where(taken, value if weighted else hot, 0.0)

    pick = selection(1 - p, False).T.astype(BF16)
    for copy in token_loads:
        copy.wait()
    tokens = xin[...].astype(F32)
    scale = lax.rsqrt(jnp.mean(tokens * tokens, axis=-1, keepdims=True) + EPS)
    normed = (tokens * scale * pre_gain[...]).astype(BF16)
    for k in range(4):
        piece = jnp.dot(pick[128 * k : 128 * k + 128], normed, preferred_element_type=F32)
        sendbuf[4 * k : 4 * k + 4] = piece.astype(BF16).reshape(4, 2, 16, 2048)

    pl.semaphore_wait(bar, 39)

    def to_plane(k, core):
        dy, dx = ORDER[k]
        return remote(
            sendbuf.at[k, core], rows_in.at[k, c], send_a.at[k, core], recv_a.at[k, c],
            (plane(dy, dx), 2 * z + core),
        )

    w_z = []
    for dz in range(1, 8):
        copy = remote(w_src, w_all.at[c, w_mine, z], send_w.at[dz], recv_w.at[dz], along(dz))
        copy.start()
        w_z.append(copy)
    for k in range(1, 16):
        for core in range(2):
            to_plane(k, core).start()
    to_mate = remote(sendbuf.at[0, 1 - c], rows_in.at[0, c], send_a.at[0, 0], recv_a.at[0, 0], mate)
    to_mate.start()
    rim = remote(pool_in.at[pl.ds(496, 16)], padded.at[pl.ds(0, 16)], send_h, recv_h, after)
    rim.start()
    swaps = [
        remote(gate_weight.at[1 - c], gate_w.at[1], send_o.at[0], recv_o.at[0], mate),
        remote(up_weight.at[1 - c], up_w.at[1], send_o.at[1], recv_o.at[1], mate),
        remote(down_weight.at[1 - c], down_w.at[1], send_o.at[2], recv_o.at[2], mate),
    ]
    for copy in swaps:
        copy.start()
    rows_in[0, c] = sendbuf[0, c]

    pool_load.wait()
    rim.wait_recv()
    number = i * 16 + j
    row = lax.broadcasted_iota(jnp.int32, (528, 1), 0)
    live = (row >= 16) | (number > 0)
    position = number * 512 + lax.broadcasted_iota(jnp.int32, (512, 1), 0)
    for g, window in enumerate(WINDOWS):
        inverse = 1.0 / jnp.minimum(position + 1, window).astype(F32)
        diffs = []
        for half in range(2):
            cols = slice(g * 256 + half * 128, g * 256 + half * 128 + 128)
            values = jnp.where(live, padded[:, cols].astype(F32), 0.0)
            total = values
            reach = 1
            while reach < window:
                total = total + pltpu.roll(total, reach, 0)
                reach *= 2
            diffs.append((total[16:] * inverse - values[16:]).astype(BF16))
        diff = jnp.concatenate(diffs, axis=1)
        out = jnp.dot(diff, pool_weight[g], preferred_element_type=F32)
        mixed[:, g * 256 : (g + 1) * 256] = (out * pool_gain[:, g * 256 : (g + 1) * 256]).astype(BF16)

    def onward(k, core):
        return remote(
            rows_in.at[k, core], rows_z.at[k, core], send_z.at[k, core], recv_z.at[k, core],
            along(1 if core == 0 else 7),
        )

    def arrive(ks):
        for k in ks:
            if k == 0:
                to_mate.wait_recv()
            for core in range(2):
                if k:
                    remote(sendbuf.at[k, core], rows_in.at[k, core], send_a.at[k, core], recv_a.at[k, core], here).wait_recv()
                onward(k, core).start()

    def experts(source, first):
        block = source[first : first + 8].reshape(256, 2048)
        hidden = []
        for half in range(2):
            gate = jnp.dot(block, gate_w[half], preferred_element_type=F32)
            up = jnp.dot(block, up_w[half], preferred_element_type=F32)
            hidden.append(clamped_unit(gate, up).astype(BF16))
        hidden = jnp.concatenate(hidden, axis=1)
        return jnp.dot(hidden, down_w[...].reshape(512, 2048), preferred_element_type=F32)

    def partial(k, core):
        return remote(
            part_in.at[k, core], neigh.at[k, core], send_p.at[k, core], recv_p.at[k, core],
            along(1 if core == 0 else 7),
        )

    def inner(first):
        part_in[first : first + 8] = experts(rows_in, first).astype(BF16).reshape(8, 2, 16, 2048)
        for k in range(first, first + 8):
            for core in range(2):
                partial(k, core).start()

    def outer(first):
        for k in range(first, first + 8):
            for core in range(2):
                onward(k, core).wait_recv()
        part_z[first : first + 8] = experts(rows_z, first).reshape(8, 2, 16, 2048)

    def w_first():
        w_load.wait()
        for copy in w_z:
            copy.wait_recv()
        for k in range(1, 4):
            w_fast(k).start()

    def w_fast(k):
        dy, dx = jnp.where(c == 0, 0, k), jnp.where(c == 0, k, 0)
        return remote(w_all.at[c, w_mine], w_all.at[c, w_mine], send_w.at[7 + k], recv_w.at[7 + k], (plane(dy, dx), j))

    def w_slow(k):
        dy, dx = jnp.where(c == 0, k, 0), jnp.where(c == 0, 0, k)
        strip = w_all.at[c, pl.ds(slow * 4, 4)]
        return remote(strip, strip, send_w.at[10 + k], recv_w.at[10 + k], (plane(dy, dx), j))

    def w_core():
        return remote(w_all.at[c], w_all.at[c], send_w.at[0], recv_w.at[0], mate)

    arrive(range(0, 4))
    w_first()
    arrive(range(4, 8))
    for copy in weight_loads:
        copy.wait()
    for copy in swaps:
        copy.wait_recv()
    inner(0)
    arrive(range(8, 12))
    outer(0)
    for k in range(1, 4):
        w_fast(k).wait_recv()
    for k in range(1, 4):
        w_slow(k).start()
    arrive(range(12, 16))
    inner(8)
    outer(8)

    def home(k, core):
        dy, dx = ORDER[k]
        return remote(
            sums.at[k, core], back.at[k, c], send_r.at[k, core], recv_r.at[k, c],
            (plane(-dy, -dx), 2 * z + core),
        )

    home_mate = remote(sums.at[0, 1 - c], back.at[0, c], send_r.at[0, 0], recv_r.at[0, 0], mate)

    def settle(ks):
        for k in ks:
            for core in range(2):
                partial(k, core).wait_recv()
            sums[k] = (part_z[k] + neigh[k].astype(F32)).astype(BF16)
            if k == 0:
                home_mate.start()
                back[0, c] = sums[0, c]
            else:
                for core in range(2):
                    home(k, core).start()

    settle(range(0, 8))
    for k in range(1, 4):
        w_slow(k).wait_recv()
    w_core().start()
    settle(range(8, 16))

    w_core().wait_recv()
    outs = []
    for h in range(2):
        rows = mixed[256 * h : 256 * h + 256]
        square = jnp.zeros((256, 1), F32)
        for n in range(8):
            sides = []
            for b in (2 * n, 2 * n + 1):
                turned = (b % 4) * 4 + b // 4
                sides.append(
                    jnp.concatenate([w_all[core, (b, turned)[core], q] for q in range(8) for core in range(2)], axis=0)
                )
            out = jnp.dot(rows, jnp.concatenate(sides, axis=1), preferred_element_type=F32)
            square = square + jnp.sum(out * out, axis=-1, keepdims=True)
            acc[:, 256 * n : 256 * n + 256] = out
        scale = lax.rsqrt(square * (1.0 / 2048.0) + EPS)
        staged[h] = (acc[...] * scale * mix_gain[...]).astype(BF16)
        copy = pltpu.make_async_copy(staged.at[h], mix_out.at[pl.ds(256 * h, 256)], out_sem.at[h])
        copy.start()
        outs.append(copy)

    weight = selection(p, True)
    high = weight.astype(BF16)
    low = (weight - high.astype(F32)).astype(BF16)
    both = jnp.concatenate([high, low], axis=0)
    home_mate.wait_recv()
    for k in range(1, 16):
        for core in range(2):
            remote(sums.at[k, core], back.at[k, core], send_r.at[k, core], recv_r.at[k, core], here).wait_recv()
    total = jnp.dot(both, back[...].reshape(512, 2048), preferred_element_type=F32)
    total = total[:64] + total[64:]
    mine[...] = total.astype(BF16).reshape(4, 16, 2048)

    def spread(m):
        return remote(
            mine.at[((z + 8 - 2 * m) % 8) // 2], theirs.at[m], send_t.at[m], recv_t.at[m], along(8 - 2 * m)
        )

    for m in (2, 1, 3):
        spread(m).start()
    acc[0:64] = total
    result = acc[pl.ds(pl.multiple_of((z // 2) * 16, 16), 16), :]
    for m in (1, 3, 2):
        spread(m).wait_recv()
        result = result + theirs[m].astype(F32)
    scale = lax.rsqrt(jnp.mean(result * result, axis=-1, keepdims=True) + EPS)
    expert_out[...] = (result * scale * post_gain[...]).astype(BF16)

    for copy in outs:
        copy.wait()
    for copy in w_z + swaps + [rim, to_mate, home_mate, w_core()]:
        copy.wait_send()
    for k in range(1, 4):
        w_fast(k).wait_send()
        w_slow(k).wait_send()
        spread(k).wait_send()
    for k in range(16):
        for core in range(2):
            onward(k, core).wait_send()
            partial(k, core).wait_send()
            if k:
                to_plane(k, core).wait_send()
                home(k, core).wait_send()


def body(
    pool_in, pool_weight, pool_gain, out_weight, mix_gain, expert_in, routes, route_weight, pre_gain,
    gate_weight, up_weight, down_weight, post_gain,
):
    vmem = pl.BlockSpec(memory_space=pltpu.VMEM)
    hbm = pl.BlockSpec(memory_space=pl.ANY)
    dma = pltpu.SemaphoreType.DMA
    tile = (16, 2, 16, 2048)
    return pl.pallas_call(
        kernel,
        out_shape=(
            jax.ShapeDtypeStruct((512, 2048), BF16),
            jax.ShapeDtypeStruct((16, 2048), BF16),
        ),
        in_specs=[hbm, vmem, vmem, hbm, vmem, hbm, vmem, vmem, vmem, hbm, hbm, hbm, vmem],
        out_specs=(hbm, vmem),
        scratch_shapes=[
            pltpu.VMEM((64, 2048), BF16),
            pltpu.VMEM(tile, BF16),
            pltpu.VMEM(tile, BF16),
            pltpu.VMEM(tile, BF16),
            pltpu.VMEM(tile, BF16),
            pltpu.VMEM(tile, F32),
            pltpu.VMEM(tile, BF16),
            pltpu.VMEM(tile, BF16),
            pltpu.VMEM(tile, BF16),
            pltpu.VMEM((4, 16, 2048), BF16),
            pltpu.VMEM((4, 16, 2048), BF16),
            pltpu.VMEM((2, 2048, 256), BF16),
            pltpu.VMEM((2, 2048, 256), BF16),
            pltpu.VMEM((2, 256, 2048), BF16),
            pltpu.VMEM((528, 1024), BF16),
            pltpu.VMEM((512, 1024), BF16),
            pltpu.VMEM((2, 16, 8, 64, 128), BF16),
            pltpu.VMEM((256, 2048), F32),
            pltpu.VMEM((2, 256, 2048), BF16),
            dma((9,)),
            dma((16, 2)), dma((16, 2)),
            dma((16, 2)), dma((16, 2)),
            dma((16, 2)), dma((16, 2)),
            dma((16, 2)), dma((16, 2)),
            dma((4,)), dma((4,)),
            dma((14,)), dma((14,)),
            dma((3,)), dma((3,)),
            dma, dma,
            dma((2,)),
        ],
        compiler_params=pltpu.CompilerParams(
            collective_id=0, has_side_effects=True, vmem_limit_bytes=60 * 1024 * 1024
        ),
        name="mixer_experts",
    )(
        pool_in, pool_weight, pool_gain.reshape(1, -1), out_weight, mix_gain.reshape(1, -1), expert_in, routes,
        route_weight, pre_gain.reshape(1, -1), gate_weight, up_weight, down_weight, post_gain.reshape(1, -1),
    )


def solution(mesh):
    return jax.shard_map(
        body,
        mesh=mesh,
        in_specs=(
            P(("ep", "tp"), None),
            P(),
            P(),
            P("tp", None),
            P(),
            P("ep", None),
            P("ep", None),
            P("ep", None),
            P(),
            P("ep", None, "tp"),
            P("ep", None, "tp"),
            P("ep", "tp", None),
            P(),
        ),
        out_specs=(P(("ep", "tp"), None), P(("ep", "tp"), None)),
        check_vma=False,
    )
```

time: 227 us -> 107 us (0.47)
  waiting for transfers between devices: 138 us -> 0 us
  Pallas kernels: 0 us -> 97.4 us
  matrix products: 29.9 us -> 0 us
  blocking collectives: 17.8 us -> 0 us
  between operations: 13.9 us -> 0.65 us
  starting transfers between devices: 8.73 us -> 0 us
  other arithmetic: 8.4 us -> 0 us
    pallas_call x0 -> x1, Pallas kernels: none -> 97.4 us  [body(): pl.pallas_call(kernel, out_shape=(jax.ShapeDtypeStruct((512, 2048), BF16)...]
    all_gather x2 -> x0, waiting for transfers between devices: 69.4 us -> none  [the longest x1 56.1 us: body(): lax.all_gather(arrived, 'tp', axis=0, tiled=True)]
    reduce_scatter x1 -> x0, waiting for transfers between devices: 62 us -> none  [body(): lax.psum_scatter(jnp.einsum('necf,efd->necd', hidden_all, down_weight, pr...]
    dot_general x6 -> x0, matrix products: 29.9 us -> none  [the longest x1 13.7 us: body(): jnp.einsum('necf,efd->necd', hidden_all, down_weight, preferred_element_t...]
    all_to_all x1 -> x0, blocking collectives: 17.8 us -> none  [body(): lax.all_to_all(buffer, 'ep', split_axis=0, concat_axis=0, tiled=True)]
    all_to_all x1 -> x0, starting transfers between devices: 6.52 us -> none  [body(): lax.all_to_all(summed, 'ep', split_axis=0, concat_axis=0, tiled=True)]
    convert_element_type x8 -> x0, other arithmetic: 5.63 us -> none  [the longest x1 3.93 us: body(): mix_out = rms_scale(projected, mix_gain).astype(jnp.bfloat16)]
    all_to_all x1 -> x0, waiting for transfers between devices: 5.31 us -> none  [body(): lax.all_to_all(summed, 'ep', split_axis=0, concat_axis=0, tiled=True)]
  transfers between devices with their start and end apart: 5 -> 0, of which waited for: 5 -> 0; matrix products, arithmetic and copies ran while one was open for 15% -> 0% of each run, Pallas kernels for 0% -> 0%
where the time goes in v1:
time: 107 us; the launch traced here: 105 us
  Pallas kernels  97.4 us (91%)
  local copies, waits for them, and re-layouts  6.79 us (6%)
    pallas_call x1, Pallas kernels, body(): pl.pallas_call(kernel, out_shape=(jax.ShapeDtypeStruct((512, 2048), BF16)...  97.4 us
    unnamed x6, local copies, waits for them, and re-layouts  6.79 us

profile of v1, /device:TPU:1, one launch (start us, length us, event | category | flops | bytes accessed | tf_op | source)
XLA Modules:
  0.0 104.8 jit_solution(17827969446885376208)
XLA Ops:
  0.6 1.5 %copy.15.routes = s32[256,4]{1,0:T(8,128)} copy(s32[256,4]{0,1:T(4,128)} %param.19) | data formatting | bytes 8192 | tf_op args[6]
  2.1 1.5 %copy.16.route_weight = f32[256,4]{1,0:T(8,128)} copy(f32[256,4]{0,1:T(4,128)} %param.20) | data formatting | bytes 8192 | tf_op args[7]
  3.6 97.4 %mixer_experts.1 = (bf16[512,2048]{1,0:T(8,128)(2,1)}, bf16[16,2048]{1,0:T(8,128)(2,1)}) custom-call(bf16[512,1024]{1,0:T(8,128)(2,1)} %pool_in.1, bf16[4,256,256]{2,1,0:T(8,128)(2,1)} %pool_weight.1, f32[1,1024]{1,0:T(1,128)} %bitcast.7, bf16[64,2048]{1,0:T(8,128)(2,1)} %out_weight.1, f32[1,2048]{1,0:T(1,128)} %bitcast.4, bf16[256,2048]{1,0:T(8,128)(2,1)} %expert_in.1, ...), custom_call_target="tpu_custom_call" | custom-call | tf_op jit(solution)/shard_map/mixer_experts/pallas_call | solution.py:368
  101.0 0.0 copy-start
  101.0 3.2 %copy.19 = bf16[512,2048]{1,0:T(8,128)(2,1)} copy(bf16[512,2048]{1,0:T(8,128)(2,1)} %get-tuple-element.4) | data formatting | bytes 4194304
  104.2 0.0 copy-done
  104.2 0.6 copy.20
Async XLA Ops:
  101.0 3.2 %copy-start = (bf16[16,2048]{1,0:T(8,128)(2,1)S(1)}, bf16[16,2048]{1,0:T(8,128)(2,1)}, u32[]{:S(2)}) copy-start(bf16[16,2048]{1,0:T(8,128)(2,1)} %get-tuple-element.5) | copy-start | bytes 196612

commit v2 on v1

--- a/solution.py
+++ b/solution.py
@@ -16,6 +16,9 @@
 BF16 = jnp.bfloat16
 
 
+phase = jax.named_scope
+
+
 def ring(a):
     return min(a, 4 - a)
 
@@ -40,9 +43,9 @@
     gate_weight, up_weight, down_weight, post_gain,
     mix_out, expert_out,
     xin, sendbuf, rows_in, rows_z, part_in, part_z, sums, neigh, back, mine, theirs,
-    gate_w, up_w, down_w, padded, mixed, w_all, acc, staged,
+    gate_w, up_w, down_w, padded, mixed, w_all, acc, table,
     local_sem, send_a, recv_a, send_z, recv_z, send_p, recv_p, send_r, recv_r, send_t, recv_t,
-    send_w, recv_w, send_o, recv_o, send_h, recv_h, out_sem,
+    send_w, recv_w, send_o, recv_o, send_h, recv_h,
 ):
     i = lax.axis_index("ep")
     j = lax.axis_index("tp")
@@ -110,9 +113,16 @@
     earlier = jnp.where((other < token) & (other // 16 == token // 16), 1.0, 0.0).astype(BF16)
     base = (lax.broadcasted_iota(jnp.int32, (64, 1), 0) // 16) * 4
 
+    def turned(ref, column):
+        block = jnp.concatenate([ref[...].astype(F32), jnp.zeros((4, 256), F32)], axis=0)
+        table[:, column : column + 8] = block.T
+
+    turned(routes, 0)
+    turned(route_weight, 8)
+
     def selection(parity, weighted):
-        chosen = jnp.concatenate([routes[pl.ds(block_row(parity, b), 16), :] for b in range(4)], axis=0)
-        weights = jnp.concatenate([route_weight[pl.ds(block_row(parity, b), 16), :] for b in range(4)], axis=0)
+        rows = jnp.concatenate([table[pl.ds(block_row(parity, b), 16), :] for b in range(4)], axis=0)
+        chosen, weights = rows[:, 0:4].astype(jnp.int32), rows[:, 8:12]
         hot = jnp.zeros((64, 512), F32)
         value = jnp.zeros((64, 512), F32)
         for k in range(4):
@@ -123,17 +133,19 @@
         taken = (rank + base) == slot_lane
         return jnp.where(taken, value if weighted else hot, 0.0)
 
-    pick = selection(1 - p, False).T.astype(BF16)
-    for copy in token_loads:
-        copy.wait()
-    tokens = xin[...].astype(F32)
-    scale = lax.rsqrt(jnp.mean(tokens * tokens, axis=-1, keepdims=True) + EPS)
-    normed = (tokens * scale * pre_gain[...]).astype(BF16)
-    for k in range(4):
-        piece = jnp.dot(pick[128 * k : 128 * k + 128], normed, preferred_element_type=F32)
-        sendbuf[4 * k : 4 * k + 4] = piece.astype(BF16).reshape(4, 2, 16, 2048)
-
-    pl.semaphore_wait(bar, 39)
+    with phase("pack"):
+        pick = selection(1 - p, False).T.astype(BF16)
+        for copy in token_loads:
+            copy.wait()
+        tokens = xin[...].astype(F32)
+        scale = lax.rsqrt(jnp.mean(tokens * tokens, axis=-1, keepdims=True) + EPS)
+        normed = (tokens * scale * pre_gain[...]).astype(BF16)
+        for k in range(4):
+            piece = jnp.dot(pick[128 * k : 128 * k + 128], normed, preferred_element_type=F32)
+            sendbuf[4 * k : 4 * k + 4] = piece.astype(BF16).reshape(4, 2, 16, 2048)
+
+    with phase("barrier"):
+        pl.semaphore_wait(bar, 39)
 
     def to_plane(k, core):
         dy, dx = ORDER[k]
@@ -163,28 +175,6 @@
         copy.start()
     rows_in[0, c] = sendbuf[0, c]
 
-    pool_load.wait()
-    rim.wait_recv()
-    number = i * 16 + j
-    row = lax.broadcasted_iota(jnp.int32, (528, 1), 0)
-    live = (row >= 16) | (number > 0)
-    position = number * 512 + lax.broadcasted_iota(jnp.int32, (512, 1), 0)
-    for g, window in enumerate(WINDOWS):
-        inverse = 1.0 / jnp.minimum(position + 1, window).astype(F32)
-        diffs = []
-        for half in range(2):
-            cols = slice(g * 256 + half * 128, g * 256 + half * 128 + 128)
-            values = jnp.where(live, padded[:, cols].astype(F32), 0.0)
-            total = values
-            reach = 1
-            while reach < window:
-                total = total + pltpu.roll(total, reach, 0)
-                reach *= 2
-            diffs.append((total[16:] * inverse - values[16:]).astype(BF16))
-        diff = jnp.concatenate(diffs, axis=1)
-        out = jnp.dot(diff, pool_weight[g], preferred_element_type=F32)
-        mixed[:, g * 256 : (g + 1) * 256] = (out * pool_gain[:, g * 256 : (g + 1) * 256]).astype(BF16)
-
     def onward(k, core):
         return remote(
             rows_in.at[k, core], rows_z.at[k, core], send_z.at[k, core], recv_z.at[k, core],
@@ -246,24 +236,6 @@
 
     def w_core():
         return remote(w_all.at[c], w_all.at[c], send_w.at[0], recv_w.at[0], mate)
-
-    arrive(range(0, 4))
-    w_first()
-    arrive(range(4, 8))
-    for copy in weight_loads:
-        copy.wait()
-    for copy in swaps:
-        copy.wait_recv()
-    inner(0)
-    arrive(range(8, 12))
-    outer(0)
-    for k in range(1, 4):
-        w_fast(k).wait_recv()
-    for k in range(1, 4):
-        w_slow(k).start()
-    arrive(range(12, 16))
-    inner(8)
-    outer(8)
 
     def home(k, core):
         dy, dx = ORDER[k]
@@ -286,62 +258,117 @@
                 for core in range(2):
                     home(k, core).start()
 
-    settle(range(0, 8))
-    for k in range(1, 4):
-        w_slow(k).wait_recv()
-    w_core().start()
-    settle(range(8, 16))
-
-    w_core().wait_recv()
-    outs = []
-    for h in range(2):
-        rows = mixed[256 * h : 256 * h + 256]
-        square = jnp.zeros((256, 1), F32)
-        for n in range(8):
-            sides = []
-            for b in (2 * n, 2 * n + 1):
-                turned = (b % 4) * 4 + b // 4
-                sides.append(
-                    jnp.concatenate([w_all[core, (b, turned)[core], q] for q in range(8) for core in range(2)], axis=0)
-                )
-            out = jnp.dot(rows, jnp.concatenate(sides, axis=1), preferred_element_type=F32)
-            square = square + jnp.sum(out * out, axis=-1, keepdims=True)
-            acc[:, 256 * n : 256 * n + 256] = out
-        scale = lax.rsqrt(square * (1.0 / 2048.0) + EPS)
-        staged[h] = (acc[...] * scale * mix_gain[...]).astype(BF16)
-        copy = pltpu.make_async_copy(staged.at[h], mix_out.at[pl.ds(256 * h, 256)], out_sem.at[h])
-        copy.start()
-        outs.append(copy)
+    def mixer_first():
+        pool_load.wait()
+        rim.wait_recv()
+        number = i * 16 + j
+        row = lax.broadcasted_iota(jnp.int32, (528, 1), 0)
+        live = (row >= 16) | (number > 0)
+        position = number * 512 + lax.broadcasted_iota(jnp.int32, (512, 1), 0)
+        for g, window in enumerate(WINDOWS):
+            inverse = 1.0 / jnp.minimum(position + 1, window).astype(F32)
+            diffs = []
+            for half in range(2):
+                cols = slice(g * 256 + half * 128, g * 256 + half * 128 + 128)
+                values = jnp.where(live, padded[:, cols].astype(F32), 0.0)
+                total = values
+                reach = 1
+                while reach < window:
+                    total = total + pltpu.roll(total, reach, 0)
+                    reach *= 2
+                diffs.append((total[16:] * inverse - values[16:]).astype(BF16))
+            diff = jnp.concatenate(diffs, axis=1)
+            out = jnp.dot(diff, pool_weight[g], preferred_element_type=F32)
+            mixed[:, g * 256 : (g + 1) * 256] = (out * pool_gain[:, g * 256 : (g + 1) * 256]).astype(BF16)
+
+    def w_strip():
+        for k in range(1, 4):
+            w_fast(k).wait_recv()
+        for k in range(1, 4):
+            w_slow(k).start()
+
+    def w_half():
+        for k in range(1, 4):
+            w_slow(k).wait_recv()
+        w_core().start()
+
+    def weights():
+        for copy in weight_loads:
+            copy.wait()
+        for copy in swaps:
+            copy.wait_recv()
+
+    def step(name, what, *args):
+        with phase(name):
+            what(*args)
+
+    step("arrive_0", arrive, range(0, 4))
+    step("w_first", w_first)
+    step("arrive_4", arrive, range(4, 8))
+    step("weights", weights)
+    step("inner_0", inner, 0)
+    step("mixer_first", mixer_first)
+    step("arrive_8", arrive, range(8, 12))
+    step("outer_0", outer, 0)
+    step("settle_0", settle, range(0, 4))
+    step("arrive_12", arrive, range(12, 16))
+    step("inner_8", inner, 8)
+    step("settle_4", settle, range(4, 8))
+    step("w_strip", w_strip)
+    step("outer_8", outer, 8)
+    step("settle_8", settle, range(8, 12))
+    step("settle_12", settle, range(12, 16))
+    step("w_half", w_half)
+
+    with phase("mixer_second"):
+        w_core().wait_recv()
+        for h in range(2):
+            rows = mixed[256 * h : 256 * h + 256]
+            square = jnp.zeros((256, 1), F32)
+            for n in range(8):
+                sides = []
+                for b in (2 * n, 2 * n + 1):
+                    turned = (b % 4) * 4 + b // 4
+                    sides.append(
+                        jnp.concatenate([w_all[core, (b, turned)[core], q] for q in range(8) for core in range(2)], axis=0)
+                    )
+                out = jnp.dot(rows, jnp.concatenate(sides, axis=1), preferred_element_type=F32)
+                square = square + jnp.sum(out * out, axis=-1, keepdims=True)
+                acc[:, 256 * n : 256 * n + 256] = out
+            scale = lax.rsqrt(square * (1.0 / 2048.0) + EPS)
+            mix_out[256 * h : 256 * h + 256] = (acc[...] * scale * mix_gain[...]).astype(BF16)
 
     weight = selection(p, True)
     high = weight.astype(BF16)
     low = (weight - high.astype(F32)).astype(BF16)
     both = jnp.concatenate([high, low], axis=0)
-    home_mate.wait_recv()
-    for k in range(1, 16):
-        for core in range(2):
-            remote(sums.at[k, core], back.at[k, core], send_r.at[k, core], recv_r.at[k, core], here).wait_recv()
-    total = jnp.dot(both, back[...].reshape(512, 2048), preferred_element_type=F32)
-    total = total[:64] + total[64:]
-    mine[...] = total.astype(BF16).reshape(4, 16, 2048)
+    with phase("back"):
+        home_mate.wait_recv()
+        for k in range(1, 16):
+            for core in range(2):
+                remote(sums.at[k, core], back.at[k, core], send_r.at[k, core], recv_r.at[k, core], here).wait_recv()
+    with phase("combine"):
+        total = jnp.dot(both, back[...].reshape(512, 2048), preferred_element_type=F32)
+        total = total[:64] + total[64:]
+        mine[...] = total.astype(BF16).reshape(4, 16, 2048)
 
     def spread(m):
         return remote(
             mine.at[((z + 8 - 2 * m) % 8) // 2], theirs.at[m], send_t.at[m], recv_t.at[m], along(8 - 2 * m)
         )
 
-    for m in (2, 1, 3):
-        spread(m).start()
-    acc[0:64] = total
-    result = acc[pl.ds(pl.multiple_of((z // 2) * 16, 16), 16), :]
-    for m in (1, 3, 2):
-        spread(m).wait_recv()
-        result = result + theirs[m].astype(F32)
+    with phase("reduce"):
+        for m in (2, 1, 3):
+            spread(m).start()
+        acc[0:64] = total
+        result = acc[pl.ds(pl.multiple_of((z // 2) * 16, 16), 16), :]
+        for m in (1, 3, 2):
+            spread(m).wait_recv()
+            result = result + theirs[m].astype(F32)
+
     scale = lax.rsqrt(jnp.mean(result * result, axis=-1, keepdims=True) + EPS)
     expert_out[...] = (result * scale * post_gain[...]).astype(BF16)
 
-    for copy in outs:
-        copy.wait()
     for copy in w_z + swaps + [rim, to_mate, home_mate, w_core()]:
         copy.wait_send()
     for k in range(1, 4):
@@ -368,11 +395,11 @@
     return pl.pallas_call(
         kernel,
         out_shape=(
-            jax.ShapeDtypeStruct((512, 2048), BF16),
-            jax.ShapeDtypeStruct((16, 2048), BF16),
+            pltpu.VMEM((512, 2048), BF16),
+            pltpu.VMEM((16, 2048), BF16),
         ),
         in_specs=[hbm, vmem, vmem, hbm, vmem, hbm, vmem, vmem, vmem, hbm, hbm, hbm, vmem],
-        out_specs=(hbm, vmem),
+        out_specs=(vmem, vmem),
         scratch_shapes=[
             pltpu.VMEM((64, 2048), BF16),
             pltpu.VMEM(tile, BF16),
@@ -392,7 +419,7 @@
             pltpu.VMEM((512, 1024), BF16),
             pltpu.VMEM((2, 16, 8, 64, 128), BF16),
             pltpu.VMEM((256, 2048), F32),
-            pltpu.VMEM((2, 256, 2048), BF16),
+            pltpu.VMEM((256, 16), F32),
             dma((9,)),
             dma((16, 2)), dma((16, 2)),
             dma((16, 2)), dma((16, 2)),
@@ -402,15 +429,14 @@
             dma((14,)), dma((14,)),
             dma((3,)), dma((3,)),
             dma, dma,
-            dma((2,)),
         ],
         compiler_params=pltpu.CompilerParams(
             collective_id=0, has_side_effects=True, vmem_limit_bytes=60 * 1024 * 1024
         ),
         name="mixer_experts",
     )(
-        pool_in, pool_weight, pool_gain.reshape(1, -1), out_weight, mix_gain.reshape(1, -1), expert_in, routes,
-        route_weight, pre_gain.reshape(1, -1), gate_weight, up_weight, down_weight, post_gain.reshape(1, -1),
+        pool_in, pool_weight, pool_gain.reshape(1, -1), out_weight, mix_gain.reshape(1, -1), expert_in, routes.T,
+        route_weight.T, pre_gain.reshape(1, -1), gate_weight, up_weight, down_weight, post_gain.reshape(1, -1),
     )
 
 

time: 107 us -> 96 us (0.90); the launches traced: 105 us -> 95.1 us
  Pallas kernels: 97.4 us -> 92.5 us
  local copies, waits for them, and re-layouts: 6.79 us -> 1.95 us
    pallas_call x1, Pallas kernels: 97.4 us -> 92.5 us  [body(): pl.pallas_call(kernel, out_shape=(pltpu.VMEM((512, 2048), BF16), pltpu.VM...]
    unnamed x6 -> x2, local copies, waits for them, and re-layouts: 6.79 us -> 1.95 us
where the time goes in v2:
time: 96 us; the launch traced here: 95.1 us
  Pallas kernels  92.5 us (96%)
  local copies, waits for them, and re-layouts  1.95 us (2%)
    pallas_call x1, Pallas kernels, body(): pl.pallas_call(kernel, out_shape=(pltpu.VMEM((512, 2048), BF16), pltpu.VM...  92.5 us
    unnamed x2, local copies, waits for them, and re-layouts  1.95 us

profile of v2, /device:TPU:1, one launch (start us, length us, event | category | flops | bytes accessed | tf_op | source)
XLA Modules:
  0.0 95.1 jit_solution(16896427879080221289)
XLA Ops:
  0.6 92.5 %mixer_experts.1 = (bf16[512,2048]{1,0:T(8,128)(2,1)S(1)}, bf16[16,2048]{1,0:T(8,128)(2,1)S(1)}) custom-call(bf16[512,1024]{1,0:T(8,128)(2,1)} %pool_in.1, bf16[4,256,256]{2,1,0:T(8,128)(2,1)} %pool_weight.1, f32[1,1024]{1,0:T(1,128)} %bitcast.9, bf16[64,2048]{1,0:T(8,128)(2,1)} %out_weight.1, f32[1,2048]{1,0:T(1,128)} %bitcast.6, ...), custom_call_target="tpu_custom_call" | custom-call | tf_op jit(solution)/shard_map/mixer_experts/pallas_call | solution.py:395
  93.1 1.3 %copy.17 = bf16[512,2048]{1,0:T(8,128)(2,1)} copy(bf16[512,2048]{1,0:T(8,128)(2,1)S(1)} %get-tuple-element.2) | data formatting | bytes 4194304
  94.4 0.6 copy.18

commit v3 on v2

v3 whole, which is shorter than its diff:
```python
import functools

import jax
import jax.numpy as jnp
from jax import lax
from jax.experimental import pallas as pl
from jax.experimental.pallas import tpu as pltpu
from jax.sharding import PartitionSpec as P

MESH = pl.DeviceIdType.MESH
WINDOWS = (2, 4, 8, 16)
EPS = 1e-06
LIMIT = 7.0
ALPHA = 1.702
F32 = jnp.float32
BF16 = jnp.bfloat16


phase = jax.named_scope


FIRST = (1, 3, 2, 0)
SECOND = (2, 1, 3, 0)
OWN = 3
OTHERS = (0, 1, 2)


def clamped_unit(gate, up):
    gate = jnp.minimum(gate, LIMIT)
    up = jnp.clip(up, -LIMIT, LIMIT)
    return (up + 1.0) * gate * jax.nn.sigmoid(ALPHA * gate)


def remote(src, dst, send, recv, device):
    return pltpu.make_async_remote_copy(
        src_ref=src, dst_ref=dst, send_sem=send, recv_sem=recv, device_id=device, device_id_type=MESH
    )


def kernel(
    pool_in, pool_weight, pool_gain, out_weight, mix_gain, expert_in, routes, route_weight, pre_gain,
    gate_weight, up_weight, down_weight, post_gain,
    mix_out, expert_out,
    pool_w, pool_g, mix_g, pre_g, post_g, routes_v, route_w,
    tokens, picks, picks_in, sendbuf, rows_in, rows_z, part_in, part_z, sums, neigh, back, homebuf, homes,
    mine, theirs, gate_w, up_w, down_w, padded, mixed, w_all, acc, table, xin, own,
    local_sem, send_k, recv_k, send_m, recv_m, send_f, recv_f, send_a, recv_a, send_z, recv_z, send_p, recv_p, send_r, recv_r, send_t, recv_t,
    send_w, recv_w, send_o, recv_o, send_h, recv_h,
):
    i = lax.axis_index("ep")
    j = lax.axis_index("tp")
    z, c = j // 2, j % 2
    y, x = i // 4, i % 4
    p = z % 2
    here = (i, j)
    mate = (i, 2 * z + 1 - c)

    def plane(dy, dx):
        return ((y + dy) % 4) * 4 + (x + dx) % 4

    def turn(da, db):
        return plane(jnp.where(c == 0, da, db), jnp.where(c == 0, db, da))

    def along(dz):
        return (i, 2 * ((z + dz) % 8) + c)

    after = (jnp.where(j == 15, (i + 1) % 16, i), (j + 1) % 16)
    before = (jnp.where(j == 0, (i + 15) % 16, i), (j + 15) % 16)

    bar = pltpu.get_barrier_semaphore()

    def greet(device):
        pl.semaphore_signal(bar, inc=1, device_id=device, device_id_type=MESH)

    for d in range(1, 4):
        for core in range(2):
            greet((plane(d, 0), 2 * z + core))
            greet((plane(0, d), 2 * z + core))
    for dz in range(1, 8):
        greet(along(dz))
    greet(mate)
    greet((jnp.where(c == 1, after[0], before[0]), jnp.where(c == 1, after[1], before[1])))

    def block_row(parity, b):
        return pl.multiple_of((2 * (parity + 2 * b) + c) * 16, 16)

    loads = []

    def load(src, dst):
        copy = pltpu.make_async_copy(src, dst, local_sem.at[len(loads)])
        copy.start()
        loads.append(copy)
        return copy

    table_loads = [load(routes, routes_v), load(route_weight, route_w)]
    token_loads = [
        load(expert_in.at[pl.ds(block_row(1 - p, b), 16)], xin.at[pl.ds(16 * b, 16)]) for b in range(4)
    ]
    token_loads.append(load(pre_gain, pre_g))
    weight_loads = [
        load(gate_weight.at[c], gate_w.at[0]),
        load(up_weight.at[c], up_w.at[0]),
        load(down_weight.at[c], down_w.at[0]),
    ]
    gain_loads = [load(mix_gain, mix_g), load(post_gain, post_g)]
    pool_loads = [load(pool_weight, pool_w), load(pool_gain, pool_g)]
    pool_load = load(pool_in, padded.at[pl.ds(16, 512)])
    slow, fast = jnp.where(c == 0, y, x), jnp.where(c == 0, x, y)
    w_mine = slow * 4 + fast
    w_src = out_weight.at[:, pl.ds(pl.multiple_of(i * 128, 128), 128)]
    w_load = load(w_src, w_all.at[c, w_mine, z])

    lane = lax.broadcasted_iota(jnp.int32, (1, 512), 1)
    expert = jnp.zeros((1, 512), jnp.int32)
    for k in range(16):
        expert = jnp.where(lane // 32 == k, 2 * turn(FIRST[k // 4], SECOND[k % 4]), expert)
    expert = expert + (lane // 16) % 2
    slot_lane = lane % 16
    token = lax.broadcasted_iota(jnp.int32, (64, 64), 0)
    other = lax.broadcasted_iota(jnp.int32, (64, 64), 1)
    earlier = jnp.where((other < token) & (other // 16 == token // 16), 1.0, 0.0).astype(BF16)
    base = (lax.broadcasted_iota(jnp.int32, (64, 1), 0) // 16) * 4

    def turned(ref, column):
        block = jnp.concatenate([ref[...].astype(F32), jnp.zeros((4, 256), F32)], axis=0)
        table[:, column : column + 8] = block.T

    for copy in table_loads:
        copy.wait()
    turned(routes_v, 0)
    turned(route_w, 8)

    def selection(parity, weighted):
        rows = jnp.concatenate([table[pl.ds(block_row(parity, b), 16), :] for b in range(4)], axis=0)
        chosen, weights = rows[:, 0:4].astype(jnp.int32), rows[:, 8:12]
        hot = jnp.zeros((64, 512), F32)
        value = jnp.zeros((64, 512), F32)
        for k in range(4):
            match = chosen[:, k : k + 1] == expert
            hot = jnp.where(match, 1.0, hot)
            value = jnp.where(match, weights[:, k : k + 1], value)
        rank = jnp.dot(earlier, hot.astype(BF16), preferred_element_type=F32).astype(jnp.int32)
        taken = (rank + base) == slot_lane
        return jnp.where(taken, value if weighted else hot, 0.0)

    def landed(ref, sem):
        remote(ref, ref, send_h, sem, here).wait_recv()

    def left(ref, sem):
        remote(ref, ref, sem, recv_h, here).wait_send()

    def fill(a):
        pick = picks_in[a, 0:64].astype(F32).T.astype(BF16)
        rows = jnp.dot(pick, tokens[a], preferred_element_type=F32)
        sendbuf[4 * a : 4 * a + 4] = rows.astype(BF16).reshape(4, 2, 16, 2048)

    with phase("pack"):
        pick = selection(1 - p, False).astype(BF16)
        weight = selection(p, True)
        high = weight.astype(BF16)
        low = (weight - high.astype(F32)).astype(BF16)
        for a in range(4):
            lanes = slice(128 * a, 128 * a + 128)
            picks[a] = jnp.concatenate([pick[:, lanes], high[:, lanes], low[:, lanes]], axis=0)
        picks_in[OWN] = picks[OWN]
        for copy in token_loads:
            copy.wait()
        values = xin[...].astype(F32)
        scale = lax.rsqrt(jnp.mean(values * values, axis=-1, keepdims=True) + EPS)
        tokens[OWN] = (values * scale * pre_g[...]).astype(BF16)
        fill(OWN)

    with phase("barrier"):
        pl.semaphore_wait(bar, 21)

    def to_axis(a):
        device = (turn(FIRST[a], 0), j)
        return [
            remote(tokens.at[OWN], tokens.at[a], send_k, recv_k.at[a], device),
            remote(picks.at[a], picks_in.at[a], send_m, recv_m.at[a], device),
        ]

    def to_plane(k, core):
        return remote(
            sendbuf.at[k, core], rows_in.at[k, c], send_a, recv_a.at[k],
            (turn(0, SECOND[k % 4]), 2 * z + core),
        )

    def to_mate(k):
        return remote(sendbuf.at[k, 1 - c], rows_in.at[k, c], send_a, recv_a.at[k], mate)

    def pack(a):
        if a != OWN:
            for copy in to_axis(a):
                copy.wait_recv()
            fill(a)
        to_mate(4 * a + OWN).start()
        for b in OTHERS:
            for core in range(2):
                to_plane(4 * a + b, core).start()
        rows_in[4 * a + OWN, c] = sendbuf[4 * a + OWN, c]

    def axis():
        for a in OTHERS:
            for copy in to_axis(a):
                copy.start()

    def w_begin():
        for copy in w_z:
            copy.start()

    w_z = []
    for dz in range(1, 8):
        copy = remote(w_src, w_all.at[c, w_mine, z], send_w.at[0], recv_w.at[0], along(dz))
        w_z.append(copy)
    rim = remote(pool_in.at[pl.ds(496, 16)], padded.at[pl.ds(0, 16)], send_h, recv_h, after)
    swaps = [
        remote(gate_weight.at[1 - c], gate_w.at[1], send_o.at[0], recv_o.at[0], mate),
        remote(up_weight.at[1 - c], up_w.at[1], send_o.at[1], recv_o.at[1], mate),
        remote(down_weight.at[1 - c], down_w.at[1], send_o.at[2], recv_o.at[2], mate),
    ]

    def onward(k, core):
        return remote(
            rows_in.at[k, core], rows_z.at[k, core], send_z, recv_z.at[k // 8],
            along(1 if core == 0 else 7),
        )

    def arrive(ks):
        for k in ks:
            if k % 4 != OWN:
                landed(rows_in.at[k], recv_a.at[k])
            else:
                landed(rows_in.at[k, 1 - c], recv_a.at[k])
            for core in range(2):
                onward(k, core).start()

    def experts(source, first, count):
        block = source[first : first + count].reshape(32 * count, 2048)
        hidden = []
        for half in range(2):
            gate = jnp.dot(block, gate_w[half], preferred_element_type=F32)
            up = jnp.dot(block, up_w[half], preferred_element_type=F32)
            hidden.append(clamped_unit(gate, up).astype(BF16))
        hidden = jnp.concatenate(hidden, axis=1)
        return jnp.dot(hidden, down_w[...].reshape(512, 2048), preferred_element_type=F32)

    def partial(k, core):
        return remote(
            part_in.at[k, core], neigh.at[k, core], send_p, recv_p.at[k],
            along(1 if core == 0 else 7),
        )

    def inner(first, count):
        part = experts(rows_in, first, count)
        part_in[first : first + count] = part.astype(BF16).reshape(count, 2, 16, 2048)
        for k in range(first, first + count):
            for core in range(2):
                partial(k, core).start()

    def outer(first, count):
        landed(rows_z.at[pl.ds(first, count)], recv_z.at[first // 8])
        part_z[first : first + count] = experts(rows_z, first, count).reshape(count, 2, 16, 2048)

    def w_first():
        w_load.wait()
        landed(w_all.at[c, w_mine, pl.ds(0, 7)], recv_w.at[0])
        for k in range(1, 4):
            w_fast(k).start()

    def w_fast(k):
        dy, dx = jnp.where(c == 0, 0, k), jnp.where(c == 0, k, 0)
        return remote(w_all.at[c, w_mine], w_all.at[c, w_mine], send_w.at[1], recv_w.at[1], (plane(dy, dx), j))

    def w_slow(k):
        dy, dx = jnp.where(c == 0, k, 0), jnp.where(c == 0, 0, k)
        strip = w_all.at[c, pl.ds(slow * 4, 4)]
        return remote(strip, strip, send_w.at[2], recv_w.at[2], (plane(dy, dx), j))

    def w_core():
        return remote(w_all.at[c], w_all.at[c], send_w.at[3], recv_w.at[3], mate)

    def home(k, core):
        step_back = -SECOND[k % 4]
        there = plane(0, step_back) if core == 0 else plane(step_back, 0)
        return remote(
            sums.at[k, core], back.at[k, c], send_r, recv_r.at[k // 4], (there, 2 * z + core)
        )

    def home_mate(k):
        return remote(sums.at[k, 1 - c], back.at[k, c], send_r, recv_r.at[k // 4], mate)

    def settle(ks):
        for k in ks:
            landed(neigh.at[k], recv_p.at[k])
            sums[k] = (part_z[k] + neigh[k].astype(F32)).astype(BF16)
            if k % 4 != OWN:
                for core in range(2):
                    home(k, core).start()
            else:
                home_mate(k).start()
                back[k, c] = sums[k, c]

    def to_home(a):
        return remote(homebuf.at[a], homes.at[a], send_f, recv_f.at[a], (turn(-FIRST[a], 0), j))

    def combine(a):
        landed(back.at[pl.ds(0, 7), 0], recv_r.at[a])
        rows = back[4 * a : 4 * a + 4].reshape(128, 2048)
        both = jnp.dot(picks_in[a, 64:192], rows, preferred_element_type=F32)
        total = both[:64] + both[64:]
        if a != OWN:
            homebuf[a] = total.astype(BF16)
            to_home(a).start()
        else:
            own[...] = total

    def mixer_first():
        for copy in pool_loads + [pool_load]:
            copy.wait()
        rim.wait_recv()
        number = i * 16 + j
        row = lax.broadcasted_iota(jnp.int32, (528, 1), 0)
        live = (row >= 16) | (number > 0)
        position = number * 512 + lax.broadcasted_iota(jnp.int32, (512, 1), 0)
        for g, window in enumerate(WINDOWS):
            inverse = 1.0 / jnp.minimum(position + 1, window).astype(F32)
            diffs = []
            for half in range(2):
                cols = slice(g * 256 + half * 128, g * 256 + half * 128 + 128)
                values = jnp.where(live, padded[:, cols].astype(F32), 0.0)
                total = values
                reach = 1
                while reach < window:
                    total = total + pltpu.roll(total, reach, 0)
                    reach *= 2
                diffs.append((total[16:] * inverse - values[16:]).astype(BF16))
            diff = jnp.concatenate(diffs, axis=1)
            out = jnp.dot(diff, pool_w[g], preferred_element_type=F32)
            mixed[:, g * 256 : (g + 1) * 256] = (out * pool_g[:, g * 256 : (g + 1) * 256]).astype(BF16)

    def w_strip():
        landed(w_all.at[c, pl.ds(0, 3)], recv_w.at[1])
        for k in range(1, 4):
            w_slow(k).start()

    def w_half():
        landed(w_all.at[c, pl.ds(0, 12)], recv_w.at[2])
        w_core().start()

    def weights():
        for copy in weight_loads:
            copy.wait()
        for copy in swaps:
            copy.wait_recv()

    def swap(n):
        swaps[n].start()

    def rim_begin():
        rim.start()

    def step(name, what, *args):
        with phase(name):
            what(*args)

    def mixer_second():
        for copy in gain_loads:
            copy.wait()
        w_core().wait_recv()
        for h in range(2):
            rows = mixed[256 * h : 256 * h + 256]
            square = jnp.zeros((256, 1), F32)
            for n in range(8):
                sides = []
                for b in (2 * n, 2 * n + 1):
                    turned = (b % 4) * 4 + b // 4
                    sides.append(
                        jnp.concatenate([w_all[core, (b, turned)[core], q] for q in range(8) for core in range(2)], axis=0)
                    )
                out = jnp.dot(rows, jnp.concatenate(sides, axis=1), preferred_element_type=F32)
                square = square + jnp.sum(out * out, axis=-1, keepdims=True)
                acc[:, 256 * n : 256 * n + 256] = out
            scale = lax.rsqrt(square * (1.0 / 2048.0) + EPS)
            mix_out[256 * h : 256 * h + 256] = (acc[...] * scale * mix_g[...]).astype(BF16)

    step("00_w_begin", w_begin)
    step("01_axis", axis)
    step("02_pack_3", pack, 3)
    step("03_rim_begin", rim_begin)
    step("04_arrive_15", arrive, (15,))
    step("05_swap_0", swap, 0)
    step("06_arrive_12_13_14", arrive, (12,13,14))
    step("07_pack_0", pack, 0)
    step("08_swap_1", swap, 1)
    step("09_pack_1", pack, 1)
    step("10_arrive_3_0_1_2", arrive, (3,0,1,2))
    step("11_swap_2", swap, 2)
    step("12_pack_2", pack, 2)
    step("13_w_first", w_first)
    step("14_arrive_7_4_5_6", arrive, (7,4,5,6))
    step("15_weights", weights)
    step("16_inner_0_8", inner, 0,8)
    step("17_arrive_11_8_9_10", arrive, (11,8,9,10))
    step("18_mixer_first", mixer_first)
    step("19_w_strip", w_strip)
    step("20_inner_8_8", inner, 8,8)
    step("21_outer_0_8", outer, 0,8)
    step("22_settle_0_1_2_3", settle, (0,1,2,3))
    step("23_settle_4_5_6_7", settle, (4,5,6,7))
    step("24_outer_8_8", outer, 8,8)
    step("25_combine_0", combine, 0)
    step("26_combine_1", combine, 1)
    step("27_w_half", w_half)
    step("28_settle_8_9_10_11", settle, (8,9,10,11))
    step("29_settle_12_13_14_15", settle, (12,13,14,15))
    step("30_combine_2", combine, 2)
    step("31_mixer_second", mixer_second)
    step("32_combine_3", combine, 3)
    with phase("home"):
        total = own[...]
        for a in OTHERS:
            to_home(a).wait_recv()
            total = total + homes[a].astype(F32)
    mine[...] = total.astype(BF16).reshape(4, 16, 2048)

    def spread(m):
        return remote(
            mine.at[((z + 8 - 2 * m) % 8) // 2], theirs.at[m], send_t, recv_t.at[m], along(8 - 2 * m)
        )

    with phase("reduce"):
        for m in (2, 1, 3):
            spread(m).start()
        own[...] = total
        result = own[pl.ds(pl.multiple_of((z // 2) * 16, 16), 16), :]
        for m in (1, 3, 2):
            spread(m).wait_recv()
            result = result + theirs[m].astype(F32)

    with phase("norm"):
        scale = lax.rsqrt(jnp.mean(result * result, axis=-1, keepdims=True) + EPS)
        expert_out[...] = (result * scale * post_g[...]).astype(BF16)

    with phase("drain"):
        for copy in swaps + [rim, w_core()]:
            copy.wait_send()
        left(tokens.at[pl.ds(0, 3)], send_k)
        left(picks.at[pl.ds(0, 3)], send_m)
        left(homebuf.at[pl.ds(0, 3)], send_f)
        left(mine.at[pl.ds(0, 3)], send_t)
        left(w_all.at[c, w_mine, pl.ds(0, 7)], send_w.at[0])
        left(w_all.at[c, pl.ds(0, 3)], send_w.at[1])
        left(w_all.at[c, pl.ds(0, 12)], send_w.at[2])
        left(sendbuf.at[pl.ds(0, 14)], send_a)
        left(rows_in, send_z)
        left(part_in, send_p)
        left(sums.at[pl.ds(0, 14)], send_r)


def body(
    pool_in, pool_weight, pool_gain, out_weight, mix_gain, expert_in, routes, route_weight, pre_gain,
    gate_weight, up_weight, down_weight, post_gain,
):
    vmem = pl.BlockSpec(memory_space=pltpu.VMEM)
    hbm = pl.BlockSpec(memory_space=pl.ANY)
    dma = pltpu.SemaphoreType.DMA
    tile = (16, 2, 16, 2048)
    return pl.pallas_call(
        kernel,
        out_shape=(
            pltpu.VMEM((512, 2048), BF16),
            pltpu.VMEM((16, 2048), BF16),
        ),
        in_specs=[hbm] * 13,
        out_specs=(vmem, vmem),
        scratch_shapes=[
            pltpu.VMEM((4, 256, 256), BF16),
            pltpu.VMEM((1, 1024), F32),
            pltpu.VMEM((1, 2048), F32),
            pltpu.VMEM((1, 2048), F32),
            pltpu.VMEM((1, 2048), F32),
            pltpu.VMEM((4, 256), jnp.int32),
            pltpu.VMEM((4, 256), F32),
            pltpu.VMEM((4, 64, 2048), BF16),
            pltpu.VMEM((4, 192, 128), BF16),
            pltpu.VMEM((4, 192, 128), BF16),
            pltpu.VMEM(tile, BF16),
            pltpu.VMEM(tile, BF16),
            pltpu.VMEM(tile, BF16),
            pltpu.VMEM(tile, BF16),
            pltpu.VMEM(tile, F32),
            pltpu.VMEM(tile, BF16),
            pltpu.VMEM(tile, BF16),
            pltpu.VMEM(tile, BF16),
            pltpu.VMEM((4, 64, 2048), BF16),
            pltpu.VMEM((4, 64, 2048), BF16),
            pltpu.VMEM((4, 16, 2048), BF16),
            pltpu.VMEM((4, 16, 2048), BF16),
            pltpu.VMEM((2, 2048, 256), BF16),
            pltpu.VMEM((2, 2048, 256), BF16),
            pltpu.VMEM((2, 256, 2048), BF16),
            pltpu.VMEM((528, 1024), BF16),
            pltpu.VMEM((512, 1024), BF16),
            pltpu.VMEM((2, 16, 8, 64, 128), BF16),
            pltpu.VMEM((256, 2048), F32),
            pltpu.VMEM((256, 16), F32),
            pltpu.VMEM((64, 2048), BF16),
            pltpu.VMEM((64, 2048), F32),
            dma((16,)),
            dma, dma((4,)),
            dma, dma((4,)),
            dma, dma((4,)),
            dma, dma((16,)),
            dma, dma((2,)),
            dma, dma((16,)),
            dma, dma((4,)),
            dma, dma((4,)),
            dma((4,)), dma((4,)),
            dma((3,)), dma((3,)),
            dma, dma,
        ],
        compiler_params=pltpu.CompilerParams(
            collective_id=0, has_side_effects=True, vmem_limit_bytes=60 * 1024 * 1024
        ),
        name="mixer_experts",
    )(
        pool_in, pool_weight, pool_gain.reshape(1, -1), out_weight, mix_gain.reshape(1, -1), expert_in, routes.T,
        route_weight.T, pre_gain.reshape(1, -1), gate_weight, up_weight, down_weight, post_gain.reshape(1, -1),
    )


def solution(mesh):
    return jax.shard_map(
        body,
        mesh=mesh,
        in_specs=(
            P(("ep", "tp"), None),
            P(),
            P(),
            P("tp", None),
            P(),
            P("ep", None),
            P("ep", None),
            P("ep", None),
            P(),
            P("ep", None, "tp"),
            P("ep", None, "tp"),
            P("ep", "tp", None),
            P(),
        ),
        out_specs=(P(("ep", "tp"), None), P(("ep", "tp"), None)),
        check_vma=False,
    )
```

time: 96 us -> 81.8 us (0.85)
  Pallas kernels: 92.5 us -> 79.1 us
    pallas_call x1, Pallas kernels: 92.5 us -> 79.1 us  [body(): pl.pallas_call(kernel, out_shape=(pltpu.VMEM((512, 2048), BF16), pltpu.VM...]
where the time goes in v3:
time: 81.8 us; the launch traced here: 81.7 us
  Pallas kernels  79.1 us (97%)
  local copies, waits for them, and re-layouts  1.95 us (2%)
    pallas_call x1, Pallas kernels, body(): pl.pallas_call(kernel, out_shape=(pltpu.VMEM((512, 2048), BF16), pltpu.VM...  79.1 us
    unnamed x2, local copies, waits for them, and re-layouts  1.95 us

profile of v3, /device:TPU:1, one launch (start us, length us, event | category | flops | bytes accessed | tf_op | source)
XLA Modules:
  0.0 81.7 jit_solution(6457727835072195995)
XLA Ops:
  0.6 79.1 %mixer_experts.1 = (bf16[512,2048]{1,0:T(8,128)(2,1)S(1)}, bf16[16,2048]{1,0:T(8,128)(2,1)S(1)}) custom-call(bf16[512,1024]{1,0:T(8,128)(2,1)} %pool_in.1, bf16[4,256,256]{2,1,0:T(8,128)(2,1)} %pool_weight.1, f32[1,1024]{1,0:T(1,128)} %bitcast.9, bf16[64,2048]{1,0:T(8,128)(2,1)} %out_weight.1, f32[1,2048]{1,0:T(1,128)} %bitcast.6, ...), custom_call_target="tpu_custom_call" | custom-call | tf_op jit(solution)/shard_map/mixer_experts/pallas_call | solution.py:469
  79.7 1.3 %copy.17 = bf16[512,2048]{1,0:T(8,128)(2,1)} copy(bf16[512,2048]{1,0:T(8,128)(2,1)S(1)} %get-tuple-element.2) | data formatting | bytes 4194304
  81.1 0.6 copy.18

commit v4 on v3

--- a/solution.py
+++ b/solution.py
@@ -23,6 +23,7 @@
 SECOND = (2, 1, 3, 0)
 OWN = 3
 OTHERS = (0, 1, 2)
+PARTS = 2
 
 
 def clamped_unit(gate, up):
@@ -304,6 +305,13 @@
     def to_home(a):
         return remote(homebuf.at[a], homes.at[a], send_f, recv_f.at[a], (turn(-FIRST[a], 0), j))
 
+    def cut(h):
+        return pl.ds(h * (2048 // PARTS), 2048 // PARTS)
+
+    def to_home_last(h):
+        part = (2, slice(None), cut(h))
+        return remote(homebuf.at[part], homes.at[part], send_f, recv_f.at[2 + h], (turn(-FIRST[2], 0), j))
+
     def combine(a):
         landed(back.at[pl.ds(0, 7), 0], recv_r.at[a])
         rows = back[4 * a : 4 * a + 4].reshape(128, 2048)
@@ -311,7 +319,8 @@
         total = both[:64] + both[64:]
         if a != OWN:
             homebuf[a] = total.astype(BF16)
-            to_home(a).start()
+            for copy in [to_home_last(h) for h in range(PARTS)] if a == 2 else [to_home(a)]:
+                copy.start()
         else:
             own[...] = total
 
@@ -413,29 +422,36 @@
     step("26_combine_1", combine, 1)
     step("27_w_half", w_half)
     step("28_settle_8_9_10_11", settle, (8,9,10,11))
-    step("29_settle_12_13_14_15", settle, (12,13,14,15))
+    step("29_settle_12_13_14", settle, (12,13,14))
     step("30_combine_2", combine, 2)
-    step("31_mixer_second", mixer_second)
+    step("31_settle_15", settle, (15,))
     step("32_combine_3", combine, 3)
+    def spread(m, h):
+        return remote(
+            mine.at[((z + 8 - 2 * m) % 8) // 2, :, cut(h)], theirs.at[m, :, cut(h)], send_t, recv_t.at[m, h],
+            along(8 - 2 * m),
+        )
+
     with phase("home"):
         total = own[...]
-        for a in OTHERS:
+        for a in range(2):
             to_home(a).wait_recv()
             total = total + homes[a].astype(F32)
-    mine[...] = total.astype(BF16).reshape(4, 16, 2048)
-
-    def spread(m):
-        return remote(
-            mine.at[((z + 8 - 2 * m) % 8) // 2], theirs.at[m], send_t, recv_t.at[m], along(8 - 2 * m)
-        )
+        own[...] = total
+        for h in range(PARTS):
+            to_home_last(h).wait_recv()
+            part = own[:, cut(h)] + homes[2, :, cut(h)].astype(F32)
+            mine[:, :, cut(h)] = part.astype(BF16).reshape(4, 16, 2048 // PARTS)
+            for m in (2, 1, 3):
+                spread(m, h).start()
+            own[:, cut(h)] = part
 
     with phase("reduce"):
-        for m in (2, 1, 3):
-            spread(m).start()
-        own[...] = total
+        mixer_second()
         result = own[pl.ds(pl.multiple_of((z // 2) * 16, 16), 16), :]
         for m in (1, 3, 2):
-            spread(m).wait_recv()
+            for h in range(PARTS):
+                spread(m, h).wait_recv()
             result = result + theirs[m].astype(F32)
 
     with phase("norm"):
@@ -510,12 +526,12 @@
             dma((16,)),
             dma, dma((4,)),
             dma, dma((4,)),
-            dma, dma((4,)),
+            dma, dma((2 + PARTS,)),
             dma, dma((16,)),
             dma, dma((2,)),
             dma, dma((16,)),
             dma, dma((4,)),
-            dma, dma((4,)),
+            dma, dma((4, PARTS)),
             dma((4,)), dma((4,)),
             dma((3,)), dma((3,)),
             dma, dma,

time: 81.8 us -> 80 us (0.978)
  Pallas kernels: 79.1 us -> 77.3 us
    pallas_call x1, Pallas kernels: 79.1 us -> 77.3 us  [body(): pl.pallas_call(kernel, out_shape=(pltpu.VMEM((512, 2048), BF16), pltpu.VM...]
where the time goes in v4:
time: 80 us; the launch traced here: 79.9 us
  Pallas kernels  77.3 us (97%)
  local copies, waits for them, and re-layouts  1.95 us (2%)
    pallas_call x1, Pallas kernels, body(): pl.pallas_call(kernel, out_shape=(pltpu.VMEM((512, 2048), BF16), pltpu.VM...  77.3 us
    unnamed x2, local copies, waits for them, and re-layouts  1.95 us

profile of v4, /device:TPU:1, one launch (start us, length us, event | category | flops | bytes accessed | tf_op | source)
XLA Modules:
  0.0 79.9 jit_solution(9273550219538764237)
XLA Ops:
  0.6 77.3 %mixer_experts.1 = (bf16[512,2048]{1,0:T(8,128)(2,1)S(1)}, bf16[16,2048]{1,0:T(8,128)(2,1)S(1)}) custom-call(bf16[512,1024]{1,0:T(8,128)(2,1)} %pool_in.1, bf16[4,256,256]{2,1,0:T(8,128)(2,1)} %pool_weight.1, f32[1,1024]{1,0:T(1,128)} %bitcast.9, bf16[64,2048]{1,0:T(8,128)(2,1)} %out_weight.1, f32[1,2048]{1,0:T(1,128)} %bitcast.6, ...), custom_call_target="tpu_custom_call" | custom-call | tf_op jit(solution)/shard_map/mixer_experts/pallas_call | solution.py:485
  77.9 1.3 %copy.17 = bf16[512,2048]{1,0:T(8,128)(2,1)} copy(bf16[512,2048]{1,0:T(8,128)(2,1)S(1)} %get-tuple-element.2) | data formatting | bytes 4194304
  79.2 0.6 copy.18

commit v5 on v4

--- a/solution.py
+++ b/solution.py
@@ -474,6 +474,17 @@
         left(sums.at[pl.ds(0, 14)], send_r)
 
 
+def write_out(mix, expert, mix_out, expert_out, sem):
+    copies = [pltpu.make_async_copy(expert, expert_out, sem.at[4])]
+    for n in range(4):
+        part = pl.ds(128 * n, 128)
+        copies.append(pltpu.make_async_copy(mix.at[part], mix_out.at[part], sem.at[n]))
+    for copy in copies:
+        copy.start()
+    for copy in copies:
+        copy.wait()
+
+
 def body(
     pool_in, pool_weight, pool_gain, out_weight, mix_gain, expert_in, routes, route_weight, pre_gain,
     gate_weight, up_weight, down_weight, post_gain,
@@ -482,7 +493,7 @@
     hbm = pl.BlockSpec(memory_space=pl.ANY)
     dma = pltpu.SemaphoreType.DMA
     tile = (16, 2, 16, 2048)
-    return pl.pallas_call(
+    mix, expert = pl.pallas_call(
         kernel,
         out_shape=(
             pltpu.VMEM((512, 2048), BF16),
@@ -544,6 +555,18 @@
         pool_in, pool_weight, pool_gain.reshape(1, -1), out_weight, mix_gain.reshape(1, -1), expert_in, routes.T,
         route_weight.T, pre_gain.reshape(1, -1), gate_weight, up_weight, down_weight, post_gain.reshape(1, -1),
     )
+    return pl.pallas_call(
+        write_out,
+        out_shape=(
+            jax.ShapeDtypeStruct((512, 2048), BF16),
+            jax.ShapeDtypeStruct((16, 2048), BF16),
+        ),
+        in_specs=[hbm, hbm],
+        out_specs=(hbm, hbm),
+        scratch_shapes=[dma((5,))],
+        compiler_params=pltpu.CompilerParams(vmem_limit_bytes=1024 * 1024),
+        name="write_out",
+    )(mix, expert)
 
 
 def solution(mesh):

time: 80 us -> 79.4 us (level)
  local copies, waits for them, and re-layouts: 1.95 us -> 0 us
  Pallas kernels: 77.3 us -> 78.6 us
    unnamed x2 -> x0, local copies, waits for them, and re-layouts: 1.95 us -> none
    pallas_call x0 -> x1, Pallas kernels: none -> 1.38 us  [body(): pl.pallas_call(write_out, out_shape=(jax.ShapeDtypeStruct((512, 2048), BF...]
where the time goes in v5:
time: 79.4 us; the launch traced here: 79.3 us
  Pallas kernels  78.6 us (99%)
    pallas_call x1, Pallas kernels, body(): pl.pallas_call(kernel, out_shape=(pltpu.VMEM((512, 2048), BF16), pltpu.VM...  77.3 us

profile of v5, /device:TPU:1, one launch (start us, length us, event | category | flops | bytes accessed | tf_op | source)
XLA Modules:
  0.0 79.3 jit_solution(6587496041953073814)
XLA Ops:
  0.6 77.3 %mixer_experts.1 = (bf16[512,2048]{1,0:T(8,128)(2,1)S(1)}, bf16[16,2048]{1,0:T(8,128)(2,1)S(1)}) custom-call(bf16[512,1024]{1,0:T(8,128)(2,1)} %pool_in.1, bf16[4,256,256]{2,1,0:T(8,128)(2,1)} %pool_weight.1, f32[1,1024]{1,0:T(1,128)} %bitcast.9, bf16[64,2048]{1,0:T(8,128)(2,1)} %out_weight.1, f32[1,2048]{1,0:T(1,128)} %bitcast.6, ...), custom_call_target="tpu_custom_call" | custom-call | tf_op jit(solution)/shard_map/mixer_experts/pallas_call | solution.py:496
  77.9 1.4 %write_out.1 = (bf16[512,2048]{1,0:T(8,128)(2,1)}, bf16[16,2048]{1,0:T(8,128)(2,1)}) custom-call(bf16[512,2048]{1,0:T(8,128)(2,1)S(1)} %get-tuple-element.4.mix, bf16[16,2048]{1,0:T(8,128)(2,1)S(1)} %get-tuple-element.5.expert), custom_call_target="tpu_custom_call" | custom-call | tf_op jit(solution)/shard_map/write_out/pallas_call | solution.py:558
